TPU v7x, 32 devices: a whole 2x2x4 slice. The times are simulated.
32 devices in a mesh: fs: 8 (over z, x), tp: 4 (over y, core).
Axes of the slice: x: 2, y: 2, z: 4, core: 2. Of those that a mesh axis runs over, the one named last changes fastest.
Arguments:
- saved_input: bfloat16 [49152, 2048], P(('fs', 'tp')), may hold values from -6 to 6
- value_cotangent: bfloat16 [49152, 1024], P(('fs', 'tp')), may hold values from -0.0546875 to 0.0546875
- decay_cotangent: bfloat16 [49152, 16], P(('fs', 'tp')), may hold values from -0.02734375 to 0.02734375
- value_master: float32 [2048, 1024], P('fs', 'tp'), may hold values from -6 to 6
- value_factor: bfloat16 [2048, 256], P('fs'), may hold values from -0.22097087 to 0.22097087
- value_mean: float32 [256, 1024], P('fs', 'tp'), may hold values from -0.625 to 0.625
- value_second: float32 [256, 1024], P('fs', 'tp'), may hold values from 0.0001 to 0.1
- decay_master: float32 [2048, 16], replicated, may hold values from -6 to 6
- decay_mean: float32 [2048, 16], replicated, may hold values from -0.625 to 0.625
- decay_second: float32 [2048, 16], replicated, may hold values from 0.001 to 0.01
Outputs:
- value_step: float32 [2048, 1024], P('fs', 'tp')
- value_new: float32 [2048, 1024], P('fs', 'tp')
- value_copy: bfloat16 [2048, 1024], P(None, 'tp')
- mean_new: float32 [256, 1024], P('fs', 'tp')
- second_new: float32 [256, 1024], P('fs', 'tp')
- decay_step: float32 [2048, 16], replicated
- decay_copy: bfloat16 [2048, 16], replicated
All inputs are finite; a program needn't handle non-finite values.
Results may differ from a plain program's by a relative error of at most 0.0004.
Values may be sent and summed in bfloat16 or wider, within the bound.
No kernel may reach another device: no remote copies, remote signals or barrier semaphores. Data moves between devices by JAX's collectives and lax.ppermute only.
A program may use at most 64 MiB of HBM per device.

v0:
```python
import jax
import jax.numpy as jnp
from jax import lax
from jax.sharding import PartitionSpec as P

D = 2048
GW = 1024
BETA_ONE = 0.9
BETA_TWO = 0.99
ADAM_EPS = 1e-08
RMS_EPS = 1e-06
LEARN_RATE = 0.05
TOKEN_DIMS = (((0,), (0,)), ((), ()))


def adam_direction(moment_one, moment_two, gradient):
    mean_new = BETA_ONE * moment_one + (1.0 - BETA_ONE) * gradient
    second_new = BETA_TWO * moment_two + (1.0 - BETA_TWO) * gradient * gradient
    return (mean_new, second_new, mean_new / (jnp.sqrt(second_new) + ADAM_EPS))


def block_sum(left_parts, right_side):
    fs_count = lax.axis_size("fs")
    result = jnp.zeros(
        (lax.axis_size("fs") * (left_parts[0].shape[1] // fs_count), right_side.shape[1]),
        jnp.float32,
    )
    for left_side in left_parts:
        result = result + lax.dot_general(
            left_side, right_side, TOKEN_DIMS, preferred_element_type=jnp.float32
        )
    row_block = lax.psum_scatter(result, "fs", scatter_dimension=0, tiled=True)
    return lax.psum_scatter(row_block, "tp", scatter_dimension=1, tiled=True)


def local(
    saved_input,
    value_cotangent,
    decay_cotangent,
    value_master,
    value_factor,
    value_mean,
    value_second,
    decay_master,
    decay_mean,
    decay_second,
):
    decay_local = lax.dot_general(
        saved_input, decay_cotangent, TOKEN_DIMS, preferred_element_type=jnp.float32
    )
    decay_grad = lax.psum(decay_local, ("fs", "tp"))
    unused_mean, unused_second, decay_step = adam_direction(decay_mean, decay_second, decay_grad)
    decay_copy = (decay_master - LEARN_RATE * decay_step).astype(jnp.bfloat16)
    factor_wide = value_factor.astype(jnp.float32)
    mapped = jnp.dot(
        saved_input,
        lax.all_gather(value_factor, "fs", axis=0, tiled=True),
        preferred_element_type=jnp.float32,
    )
    high_part = lax.optimization_barrier(mapped.astype(jnp.bfloat16))
    low_part = (mapped - high_part.astype(jnp.float32)).astype(jnp.bfloat16)
    projected = block_sum((high_part, low_part), value_cotangent)
    mean_new, second_new, direction = adam_direction(value_mean, value_second, projected)
    raw_update = jnp.dot(
        factor_wide,
        lax.all_gather(direction, "fs", axis=0, tiled=True),
        precision=lax.Precision.HIGHEST,
        preferred_element_type=jnp.float32,
    )
    squares = lax.psum(jnp.sum(raw_update * raw_update), ("fs", "tp"))
    value_step = raw_update * lax.rsqrt(squares / (D * GW) + RMS_EPS)
    value_new = value_master - LEARN_RATE * value_step
    value_copy = lax.all_gather(value_new.astype(jnp.bfloat16), "fs", axis=0, tiled=True)
    return (value_step, value_new, value_copy, mean_new, second_new, decay_step, decay_copy)


def solution(mesh):
    in_specs = (
        P(("fs", "tp"), None),
        P(("fs", "tp"), None),
        P(("fs", "tp"), None),
        P("fs", "tp"),
        P("fs", None),
        P("fs", "tp"),
        P("fs", "tp"),
        P(),
        P(),
        P(),
    )
    out_specs = (
        P("fs", "tp"),
        P("fs", "tp"),
        P(None, "tp"),
        P("fs", "tp"),
        P("fs", "tp"),
        P(),
        P(),
    )
    return jax.shard_map(local, mesh=mesh, in_specs=in_specs, out_specs=out_specs, check_vma=False)
```

profile of v0, /device:TPU:0, one launch (start us, length us, event | category | flops | bytes accessed | tf_op | source)
XLA Modules:
  0.0 273.7 jit_solution(16057867461915626292)
XLA Ops:
  8.0 0.0 copy-start
  8.0 0.0 all-gather.3.cloned.1.call-start
  8.1 0.7 all-gather.3.cloned.1.call-update
  8.7 0.0 reduce-scatter.3.cloned.1.call-start
  8.8 45.2 %all-gather.3.cloned.1.call-done = bf16[2048,256]{1,0:T(8,128)(2,1)} async-done(((bf16[256,256]{1,0:T(8,128)(2,1)}), bf16[2048,256]{1,0:T(8,128)(2,1)}) %all-gather.3.cloned.1.call-update) | async-done | bytes 1048592 | tf_op jit(solution)/shard_map/all_gather | solution.py:57
  54.0 5.0 %fusion.8 = (bf16[1536,256]{1,0:T(8,128)(2,1)S(1)}, f32[1536,256]{1,0:T(8,128)S(1)}) fusion(bf16[1536,2048]{1,0:T(8,128)(2,1)} %param.10, bf16[2048,256]{1,0:T(8,128)(2,1)} %all-gather.3.cloned.1.call-done), kind=kOutput, calls=%fused_computation.16 | convolution fusion | flops 1611005952 | bytes 9699328 | tf_op jit(solution)/shard_map/dot_general | solution.py:55
  59.0 0.0 copy-done
  59.0 1.0 fusion.9
  60.0 0.0 copy-start.2
  60.0 2.0 convolution_add_fusion
  62.1 0.0 reduce-scatter.3.cloned.1.call-update
  62.1 0.0 reduce-scatter.5.cloned.1.call-start
  62.1 63.1 %reduce-scatter.3.cloned.1.call-done = f32[32,1024]{1,0:T(8,128)} async-done(((f32[256,1024]{1,0:T(8,128)}), f32[32,1024]{1,0:T(8,128)}) %reduce-scatter.3.cloned.1.call-update) | async-done | bytes 131088 | tf_op jit(solution)/shard_map/reduce_scatter | solution.py:32
  125.2 0.0 reduce-scatter.5.cloned.1.call-update
  125.2 0.0 copy-start.1
  125.2 0.0 all-reduce.2.cloned.1.call-start
  125.3 0.0 copy-done.2
  125.3 4.4 %fusion.10 = f32[2048,16]{0,1:T(8,128)} fusion(bf16[1536,16]{0,1:T(8,128)(2,1)S(1)} %copy-done.2, bf16[1536,2048]{1,0:T(8,128)(2,1)} %param.10), kind=kOutput, calls=%fused_computation.18 | convolution fusion | flops 100663296 | bytes 6471680 | tf_op jit(solution)/shard_map/dot_general | solution.py:48
  129.7 0.0 all-reduce.2.cloned.1.call-update
  129.7 0.0 all-gather.5.cloned.1.call-start
  129.8 1.1 copy.17
  130.8 15.4 %reduce-scatter.5.cloned.1.call-done = f32[32,256]{1,0:T(8,128)} async-done(((f32[32,1024]{1,0:T(8,128)}), f32[32,256]{1,0:T(8,128)}) %reduce-scatter.5.cloned.1.call-update) | async-done | bytes 32784 | tf_op jit(solution)/shard_map/reduce_scatter | solution.py:33
  146.3 1.4 add_divide_fusion
  147.7 30.8 %all_gather.10 = f32[256,256]{1,0:T(8,128)S(1)} all-gather(f32[32,256]{1,0:T(8,128)S(1)} %get-tuple-element.19), channel_id=1, replica_groups=mesh['fs'=8,'tp'=4] {'fs'}, dimensions={0}, use_global_device_ids=true | all-gather | bytes 294912 | tf_op jit(solution)/shard_map/all_gather | solution.py:66
  178.5 0.0 copy-done.1
  178.5 1.7 multiply_reduce_fusion
  180.2 38.8 %psum.14 = f32[]{:T(128)} all-reduce(f32[]{:T(128)} %get-tuple-element.24), channel_id=1, replica_groups=mesh['fs'=8,'tp'=4] {'fs','tp'}, use_global_device_ids=true, to_apply=%region_3.0 | all-reduce | flops 1 | bytes 8 | tf_op jit(solution)/shard_map/psum | solution.py:70
  219.7 1.8 fusion.6
  221.6 0.0 all-gather.5.cloned.1.call-update
  221.6 37.3 %all-reduce.2.cloned.1.call-done = f32[2048,16]{0,1:T(8,128)} async-done(((f32[2048,16]{0,1:T(8,128)}), f32[2048,16]{0,1:T(8,128)}) %all-reduce.2.cloned.1.call-update) | async-done | bytes 131088 | tf_op jit(solution)/shard_map/psum | solution.py:51
  258.9 1.9 subtract_convert_fusion.2
  260.7 1.8 copy.18
  262.5 1.8 copy.19
  264.3 0.0 all-gather.5.cloned.1.call-done
  264.3 2.3 copy.20
Async XLA Ops:
  8.0 51.0 %copy-start = (bf16[1536,1024]{1,0:T(8,128)(2,1)S(1)}, bf16[1536,1024]{1,0:T(8,128)(2,1)}, u32[]{:S(2)}) copy-start(bf16[1536,1024]{1,0:T(8,128)(2,1)} %param.11) | copy-start | bytes 9437188
  8.0 46.0 %all-gather.3.cloned.1.call-start = ((), (), s32[]{:S(2)}) async-start(), calls=%async_computation.2 | async-start | bytes 1179648 | tf_op jit(solution)/shard_map/all_gather | solution.py:57
  8.7 116.5 %reduce-scatter.3.cloned.1.call-start = ((), (), s32[]{:S(2)}) async-start(), calls=%async_computation.3 | async-start | bytes 1179648 | tf_op jit(solution)/shard_map/reduce_scatter | solution.py:32
  60.0 65.3 %copy-start.2 = (bf16[1536,16]{0,1:T(8,128)(2,1)S(1)}, bf16[1536,16]{0,1:T(8,128)(2,1)}, u32[]{:S(2)}) copy-start(bf16[1536,16]{0,1:T(8,128)(2,1)} %param.12) | copy-start | bytes 147460
  62.1 84.2 %reduce-scatter.5.cloned.1.call-start = ((), (), s32[]{:S(2)}) async-start(), calls=%async_computation.4 | async-start | bytes 163840 | tf_op jit(solution)/shard_map/reduce_scatter | solution.py:33
  125.2 53.3 %copy-start.1 = (bf16[256,256]{1,0:T(8,128)(2,1)S(1)}, bf16[256,256]{1,0:T(8,128)(2,1)}, u32[]{:S(2)}) copy-start(bf16[256,256]{1,0:T(8,128)(2,1)} %param.14) | copy-start | bytes 393220
  125.2 133.6 %all-reduce.2.cloned.1.call-start = ((), (), s32[]{:S(2)}) async-start(), calls=%async_computation.6 | async-start | bytes 262144 | tf_op jit(solution)/shard_map/psum | solution.py:51
  129.7 134.6 %all-gather.5.cloned.1.call-start = ((), (), s32[]{:S(2)}) async-start(), calls=%async_computation.5 | async-start | bytes 1179648 | tf_op jit(solution)/shard_map/all_gather | solution.py:73
Sparse Core Ops, SparseCore 0:
  10.9 42.9 all-gather.2
  62.2 62.9 reduce-scatter.2
  127.6 18.6 reduce-scatter.4
  221.7 41.0 all-gather.4
Sparse Core Ops, SparseCore 1:
  131.9 127.0 all-reduce.1
where the time goes:
time: 274 us
  waiting for transfers between devices  162 us (59%)
  blocking collectives  69.6 us (25%)
  between operations  16 us (6%)
  matrix products  14.1 us (5%)
  local copies, waits for them, and re-layouts  6.93 us (3%)
  other arithmetic  5.11 us (2%)
    reduce_scatter x1, waiting for transfers between devices, block_sum(): row_block = lax.psum_scatter(result, 'fs', scatter_dimension=0, tiled=True)  63.1 us
    all_gather x1, waiting for transfers between devices, local(): lax.all_gather(value_factor, 'fs', axis=0, tiled=True)  45.2 us
    psum x1, blocking collectives, local(): squares = lax.psum(jnp.sum(raw_update * raw_update), ('fs', 'tp'))  38.8 us
    psum x1, waiting for transfers between devices, local(): decay_grad = lax.psum(decay_local, ('fs', 'tp'))  37.3 us
    all_gather x1, blocking collectives, local(): lax.all_gather(direction, 'fs', axis=0, tiled=True)  30.8 us
    reduce_scatter x1, waiting for transfers between devices, block_sum(): return lax.psum_scatter(row_block, 'tp', scatter_dimension=1, tiled=True)  15.4 us
    unnamed x10, local copies, waits for them, and re-layouts  6.93 us
  transfers between devices with their start and end apart: 5, of which 4 were waited for; matrix products, arithmetic and copies ran while one was open for 6% of the time, Pallas kernels for 0%

commit v1 on v0

--- a/solution.py
+++ b/solution.py
@@ -1,3 +1,4 @@
+import functools
 import jax
 import jax.numpy as jnp
 from jax import lax
@@ -11,6 +12,24 @@
 RMS_EPS = 1e-06
 LEARN_RATE = 0.05
 TOKEN_DIMS = (((0,), (0,)), ((), ()))
+
+
+def handle_run_here(local_values, chip_axis):
+    p_next, taken_in = (jax.lax.axis_size(chip_axis), jax.lax.axis_index(chip_axis))
+    built, latest = (local_values, 1)
+    while latest < p_next:
+        rows = []
+        for t in range(p_next):
+            rows.append((t, t ^ latest))
+        newest = jax.lax.ppermute(built, chip_axis, rows)
+        piece_now = jnp.concatenate([built, newest], axis=0)
+        later = jnp.concatenate([newest, built], axis=0)
+        built = jnp.where(taken_in & latest == 0, piece_now, later)
+        latest = 2 * latest
+    return built
+
+
+turn_the_vector = functools.partial(handle_run_here, chip_axis="fs")
 
 
 def adam_direction(moment_one, moment_two, gradient):
@@ -63,7 +82,7 @@
     mean_new, second_new, direction = adam_direction(value_mean, value_second, projected)
     raw_update = jnp.dot(
         factor_wide,
-        lax.all_gather(direction, "fs", axis=0, tiled=True),
+        turn_the_vector(direction),
         precision=lax.Precision.HIGHEST,
         preferred_element_type=jnp.float32,
     )

time: 274 us -> 305 us (1.11)
  waiting for transfers between devices: 162 us -> 216 us
  blocking collectives: 69.6 us -> 39.3 us
  starting transfers between devices: 0.2 us -> 5.58 us
    psum x1, waiting for transfers between devices: 37.3 us -> 80.6 us  [local(): decay_grad = lax.psum(decay_local, ('fs', 'tp'))]
    all_gather x1 -> x0, blocking collectives: 30.8 us -> none  [local(): lax.all_gather(direction, 'fs', axis=0, tiled=True)]
    reduce_scatter x1, waiting for transfers between devices: 15.4 us -> 21 us  [block_sum(): return lax.psum_scatter(row_block, 'tp', scatter_dimension=1, tiled=True)]
    ppermute x0 -> x3, starting transfers between devices: none -> 5.38 us  [handle_run_here(): newest = jax.lax.ppermute(built, chip_axis, rows)]
    ppermute x0 -> x3, waiting for transfers between devices: none -> 5.26 us  [handle_run_here(): newest = jax.lax.ppermute(built, chip_axis, rows)]
    unnamed x10 -> x14, local copies, waits for them, and re-layouts: 6.93 us -> 6.94 us
  transfers between devices with their start and end apart: 5 -> 8, of which waited for: 4 -> 6; matrix products, arithmetic and copies ran while one was open for 6% -> 5% of each run, Pallas kernels for 0% -> 0%
where the time goes in v1:
time: 305 us
  waiting for transfers between devices  216 us (71%)
  blocking collectives  39.3 us (13%)
  between operations  16 us (5%)
  matrix products  15.2 us (5%)
  local copies, waits for them, and re-layouts  6.94 us (2%)
  other arithmetic  5.75 us (2%)
  starting transfers between devices  5.58 us (2%)
    psum x1, waiting for transfers between devices, local(): decay_grad = lax.psum(decay_local, ('fs', 'tp'))  80.6 us
    reduce_scatter x1, waiting for transfers between devices, block_sum(): row_block = lax.psum_scatter(result, 'fs', scatter_dimension=0, tiled=True)  63.1 us
    all_gather x1, waiting for transfers between devices, local(): lax.all_gather(value_factor, 'fs', axis=0, tiled=True)  45.2 us
    psum x1, blocking collectives, local(): squares = lax.psum(jnp.sum(raw_update * raw_update), ('fs', 'tp'))  39.3 us
    reduce_scatter x1, waiting for transfers between devices, block_sum(): return lax.psum_scatter(row_block, 'tp', scatter_dimension=1, tiled=True)  21 us
    unnamed x14, local copies, waits for them, and re-layouts  6.94 us
  transfers between devices with their start and end apart: 8, of which 6 were waited for; matrix products, arithmetic and copies ran while one was open for 5% of the time, Pallas kernels for 0%

profile of v1, /device:TPU:0, one launch (start us, length us, event | category | flops | bytes accessed | tf_op | source)
XLA Modules:
  0.0 304.6 jit_solution(4708726695929272078)
XLA Ops:
  8.0 0.0 copy-start
  8.0 0.0 all-gather.3.cloned.1.call-start
  8.1 0.7 all-gather.3.cloned.1.call-update
  8.7 0.0 reduce-scatter.3.cloned.1.call-start
  8.8 45.2 %all-gather.3.cloned.1.call-done = bf16[2048,256]{1,0:T(8,128)(2,1)} async-done(((bf16[256,256]{1,0:T(8,128)(2,1)}), bf16[2048,256]{1,0:T(8,128)(2,1)}) %all-gather.3.cloned.1.call-update) | async-done | bytes 1048592 | tf_op jit(solution)/shard_map/all_gather | solution.py:76
  54.0 5.0 %fusion.16 = (bf16[1536,256]{1,0:T(8,128)(2,1)S(1)}, f32[1536,256]{1,0:T(8,128)S(1)}) fusion(bf16[1536,2048]{1,0:T(8,128)(2,1)} %param.10, bf16[2048,256]{1,0:T(8,128)(2,1)} %all-gather.3.cloned.1.call-done), kind=kOutput, calls=%fused_computation.27 | convolution fusion | flops 1611005952 | bytes 9699328 | tf_op jit(solution)/shard_map/dot_general | solution.py:74
  59.0 0.0 copy-done
  59.0 1.0 fusion.17
  60.0 0.0 copy-start.3
  60.0 0.0 copy-start.4
  60.0 0.0 copy-start.2
  60.0 2.0 convolution_add_fusion
  62.1 0.0 reduce-scatter.3.cloned.1.call-update
  62.1 0.0 reduce-scatter.5.cloned.1.call-start
  62.1 63.1 %reduce-scatter.3.cloned.1.call-done = f32[32,1024]{1,0:T(8,128)} async-done(((f32[256,1024]{1,0:T(8,128)}), f32[32,1024]{1,0:T(8,128)}) %reduce-scatter.3.cloned.1.call-update) | async-done | bytes 131088 | tf_op jit(solution)/shard_map/reduce_scatter | solution.py:51
  125.2 0.0 reduce-scatter.5.cloned.1.call-update
  125.3 0.0 all-reduce.2.cloned.1.call-start
  125.3 21.0 %reduce-scatter.5.cloned.1.call-done = f32[32,256]{1,0:T(8,128)} async-done(((f32[32,1024]{1,0:T(8,128)}), f32[32,256]{1,0:T(8,128)}) %reduce-scatter.5.cloned.1.call-update) | async-done | bytes 32784 | tf_op jit(solution)/shard_map/reduce_scatter | solution.py:52
  146.3 0.0 copy-done.3
  146.3 0.0 copy-done.4
  146.3 1.4 add_divide_fusion
  147.7 1.5 collective-permute-start
  149.2 2.5 collective-permute-done
  151.6 1.5 collective-permute-start.1
  153.2 2.8 collective-permute-done.1
  156.0 0.7 maximum_select_fusion.2
  156.6 0.0 copy-start.1
  156.6 2.4 collective-permute-start.2
  159.0 0.0 copy-done.2
  159.0 4.4 %fusion.18 = f32[2048,16]{0,1:T(8,128)} fusion(bf16[1536,16]{0,1:T(8,128)(2,1)S(1)} %copy-done.2, bf16[1536,2048]{1,0:T(8,128)(2,1)} %param.10), kind=kOutput, calls=%fused_computation.29 | convolution fusion | flops 100663296 | bytes 6471680 | tf_op jit(solution)/shard_map/dot_general | solution.py:67
  163.4 0.0 all-reduce.2.cloned.1.call-update
  163.4 0.0 all-gather.5.cloned.1.call-start
  163.5 1.1 copy.17
  164.6 0.0 collective-permute-done.2
  164.6 0.0 copy-done.1
  164.6 2.8 multiply_reduce_fusion
  167.4 39.3 %psum.14 = f32[]{:T(128)} all-reduce(f32[]{:T(128)} %get-tuple-element.24), channel_id=1, replica_groups=mesh['fs'=8,'tp'=4] {'fs','tp'}, use_global_device_ids=true, to_apply=%region_3.4 | all-reduce | flops 1 | bytes 8 | tf_op jit(solution)/shard_map/psum | solution.py:89
  207.4 1.8 fusion.14
  209.2 0.0 all-gather.5.cloned.1.call-update
  209.3 80.6 %all-reduce.2.cloned.1.call-done = f32[2048,16]{0,1:T(8,128)} async-done(((f32[2048,16]{0,1:T(8,128)}), f32[2048,16]{0,1:T(8,128)}) %all-reduce.2.cloned.1.call-update) | async-done | bytes 131088 | tf_op jit(solution)/shard_map/psum | solution.py:70
  289.8 1.9 subtract_convert_fusion.2
  291.7 1.8 copy.18
  293.5 1.8 copy.19
  295.2 0.0 all-gather.5.cloned.1.call-done
  295.3 2.3 copy.20
  (1 shorter events, 0.0 us)
Async XLA Ops:
  8.0 51.0 %copy-start = (bf16[1536,1024]{1,0:T(8,128)(2,1)S(1)}, bf16[1536,1024]{1,0:T(8,128)(2,1)}, u32[]{:S(2)}) copy-start(bf16[1536,1024]{1,0:T(8,128)(2,1)} %param.11) | copy-start | bytes 9437188
  8.0 46.0 %all-gather.3.cloned.1.call-start = ((), (), s32[]{:S(2)}) async-start(), calls=%async_computation.2 | async-start | bytes 1179648 | tf_op jit(solution)/shard_map/all_gather | solution.py:76
  8.7 116.5 %reduce-scatter.3.cloned.1.call-start = ((), (), s32[]{:S(2)}) async-start(), calls=%async_computation.3 | async-start | bytes 1179648 | tf_op jit(solution)/shard_map/reduce_scatter | solution.py:51
  60.0 86.3 %copy-start.3 = (f32[32,256]{1,0:T(8,128)S(1)}, f32[32,256]{1,0:T(8,128)}, u32[]{:S(2)}) copy-start(f32[32,256]{1,0:T(8,128)} %param.16) | copy-start | bytes 98308
  60.0 86.3 %copy-start.4 = (f32[32,256]{1,0:T(8,128)S(1)}, f32[32,256]{1,0:T(8,128)}, u32[]{:S(2)}) copy-start(f32[32,256]{1,0:T(8,128)} %param.15) | copy-start | bytes 98308
  60.0 99.0 %copy-start.2 = (bf16[1536,16]{0,1:T(8,128)(2,1)S(1)}, bf16[1536,16]{0,1:T(8,128)(2,1)}, u32[]{:S(2)}) copy-start(bf16[1536,16]{0,1:T(8,128)(2,1)} %param.12) | copy-start | bytes 147460
  62.1 84.2 %reduce-scatter.5.cloned.1.call-start = ((), (), s32[]{:S(2)}) async-start(), calls=%async_computation.4 | async-start | bytes 163840 | tf_op jit(solution)/shard_map/reduce_scatter | solution.py:52
  125.3 164.6 %all-reduce.2.cloned.1.call-start = ((), (), s32[]{:S(2)}) async-start(), calls=%async_computation.6 | async-start | bytes 262144 | tf_op jit(solution)/shard_map/psum | solution.py:70
  147.7 3.9 %collective-permute-start = (f32[32,256]{1,0:T(8,128)S(1)}, f32[32,256]{1,0:T(8,128)S(1)}, u32[]{:S(2)}, u32[]{:S(2)}) collective-permute-start(f32[32,256]{1,0:T(8,128)S(1)} %get-tuple-element.19), channel_id=1, source_target_pairs={{0,4},{4,0},{8,12},{12,8},{16,20},{20,16},{24,28},{28,24},{1,5},{5... | collective-permute-start | bytes 98312 | tf_op jit(solution)/shard_map/ppermute | solution.py:24
  151.6 4.3 %collective-permute-start.1 = (f32[64,256]{1,0:T(8,128)S(1)}, f32[64,256]{1,0:T(8,128)S(1)}, u32[]{:S(2)}, u32[]{:S(2)}) collective-permute-start(f32[64,256]{1,0:T(8,128)S(1)} %maximum_select_fusion.3), channel_id=1, source_target_pairs={{0,8},{4,12},{8,0},{12,4},{16,24},{20,28},{24,16},{28,20},{1,9},{5... | collective-permute-start | bytes 196616 | tf_op jit(solution)/shard_map/ppermute | solution.py:24
  156.6 7.9 %copy-start.1 = (bf16[256,256]{1,0:T(8,128)(2,1)S(1)}, bf16[256,256]{1,0:T(8,128)(2,1)}, u32[]{:S(2)}) copy-start(bf16[256,256]{1,0:T(8,128)(2,1)} %param.14) | copy-start | bytes 393220
  156.6 7.9 %collective-permute-start.2 = (f32[128,256]{1,0:T(8,128)}, f32[128,256]{1,0:T(8,128)}, u32[]{:S(2)}, u32[]{:S(2)}) collective-permute-start(f32[128,256]{1,0:T(8,128)} %maximum_select_fusion.2), channel_id=1, source_target_pairs={{0,16},{4,20},{8,24},{12,28},{16,0},{20,4},{24,8},{28,12},{1,17},{... | collective-permute-start | bytes 393224 | tf_op jit(solution)/shard_map/ppermute | solution.py:24
  163.4 131.8 %all-gather.5.cloned.1.call-start = ((), (), s32[]{:S(2)}) async-start(), calls=%async_computation.5 | async-start | bytes 1179648 | tf_op jit(solution)/shard_map/all_gather | solution.py:92
Sparse Core Ops, SparseCore 0:
  10.9 42.9 all-gather.2
  62.2 62.9 reduce-scatter.2
  127.7 18.5 reduce-scatter.4
  209.4 40.0 all-gather.4
Sparse Core Ops, SparseCore 1:
  163.5 126.2 all-reduce.1
